TPU v7x, 128 devices: a whole 4x4x4 slice. The times are simulated.
128 devices in a mesh: fs: 16 (over z, x), tp: 8 (over y, core).
Axes of the slice: x: 4, y: 4, z: 4, core: 2. Of those that a mesh axis runs over, the one named last changes fastest.
Arguments:
- tokens: bfloat16 [16384, 2048], P(('fs', 'tp')), may hold values from -6 to 6
- mix_gain: float32 [2048], replicated, may hold values from 0.1 to 1.9
- ffn_gain: float32 [2048], replicated, may hold values from 0.1 to 1.9
- u_weight: float32 [2048, 2048], P('fs', 'tp'), may hold values from -0.125 to 0.125
- u_scale: float32 [2048], P('tp'), may hold values from 0.5 to 2
- v_weight: float32 [2048, 2048], P('fs', 'tp'), may hold values from -0.125 to 0.125
- v_scale: float32 [2048], P('tp'), may hold values from 0.3 to 12
- v_gain: float32 [2048], P('tp'), may hold values from 0.1 to 1.9
- spatial_weight: bfloat16 [8, 128, 128], replicated, may hold values from -0.5 to 0.5
- spatial_bias: float32 [8, 128], replicated, may hold values from 0.1 to 1.9
- out_weight: float32 [2048, 2048], P('tp', 'fs'), may hold values from -0.125 to 0.125
- out_scale: float32 [2048], P('fs'), may hold values from 0.5 to 2
- gate_weight: float32 [2048, 6144], P('fs', 'tp'), may hold values from -0.125 to 0.125
- gate_scale: float32 [6144], P('tp'), may hold values from 0.5 to 2
- up_weight: float32 [2048, 6144], P('fs', 'tp'), may hold values from -0.125 to 0.125
- up_scale: float32 [6144], P('tp'), may hold values from 0.5 to 2
- down_weight: float32 [6144, 2048], P('tp', 'fs'), may hold values from -0.078125 to 0.078125
- down_scale: float32 [2048], P('fs'), may hold values from 0.5 to 2
Outputs:
- layer_out: bfloat16 [16384, 2048], P(('fs', 'tp'))
All inputs are finite; a program needn't handle non-finite values.
Results may differ from a plain program's by a relative error of at most 0.02.
Values may be sent and summed in bfloat16 or wider, within the bound.
A program may use at most 64 MiB of HBM per device.

v0:
```python
import jax
import jax.numpy as jnp
from jax import lax
from jax.sharding import Mesh
from jax.sharding import PartitionSpec as P

A = 2048
A_GROUPS = 8
BLK = 128
TP = ("tp_0", "tp_1")
FS_TP = ("fs", "tp_0", "tp_1")


def copy_for_each(value, axis):
    peers = lax.axis_size(axis)
    return lax.all_to_all(
        jnp.broadcast_to(value[None], (peers, *value.shape)), axis, 0, 0, tiled=True
    )


def laid_out(tiles, dim):
    dims = list(tiles.shape[1:])
    dims[dim] *= tiles.shape[0]
    return jnp.moveaxis(tiles, 0, dim).reshape(dims)


def gather_axes(value, axes, dim):
    far, near = axes
    tiles = copy_for_each(copy_for_each(value, far), near)
    return laid_out(tiles.swapaxes(0, 1).reshape(-1, *value.shape), dim)


def split_up(value, dim, peers):
    dims = value.shape
    tiles = value.reshape(*dims[:dim], peers, dims[dim] // peers, *dims[dim + 1 :])
    return jnp.moveaxis(tiles, dim, 0)


def sent_and_summed(value, axis, dim):
    tiles = split_up(value, dim, lax.axis_size(axis))
    arrived = lax.all_to_all(tiles, axis, split_axis=0, concat_axis=0, tiled=True)
    return arrived.astype(jnp.float32).sum(axis=0)


def sum_in_two_steps(value, axes, dim):
    far, near = axes
    own = sent_and_summed(split_up(value, dim, lax.axis_size(far)), near, dim + 1)
    return jnp.sum(
        lax.all_to_all(own.astype(jnp.bfloat16), far, 0, 0, tiled=True).astype(jnp.float32), axis=0
    )


def turned_gather(arrays, axis, dims):
    turned = [jnp.moveaxis(a, dim, 0) for a, dim in zip(arrays, dims)]
    both = jnp.concatenate([t.reshape(len(t), -1) for t in turned], axis=1)
    out, at, finished = (lax.all_gather(both, axis, axis=0, tiled=True), 0, [])
    for t, dim in zip(turned, dims):
        piece = out[:, at : at + t[0].size].reshape(-1, *t.shape[1:])
        finished.append(jnp.moveaxis(piece, 0, dim))
        at += t[0].size
    return tuple(finished)


def of_everyone(value, axis):
    return copy_for_each(value, axis).sum(axis=0)


def packed_total(arrays, axis):
    ravelled, at, finished = (jnp.concatenate([a.reshape(-1) for a in arrays]), 0, [])
    running = of_everyone(ravelled, axis)
    for a in arrays:
        finished.append(running[at : at + a.size].reshape(a.shape))
        at += a.size
    return tuple(finished)


def rms_rows(values, norm_gain):
    widened = values.astype(jnp.float32)
    factor = lax.rsqrt(jnp.mean(widened * widened, axis=1, keepdims=True) + 1e-06)
    return (widened * factor * norm_gain).astype(jnp.bfloat16)


def collect_rows(shard_rows, project):
    return project(gather_axes(shard_rows, ("tp_0", "tp_1"), 0), jnp.int32(0))


def reduce_rows(term_fn, local_rows):
    return sum_in_two_steps(
        term_fn(jnp.int32(0), local_rows * lax.axis_size(TP)).astype(jnp.bfloat16),
        ("tp_0", "tp_1"),
        0,
    )


def local(
    tokens,
    mix_gain,
    ffn_gain,
    u_weight,
    u_scale,
    v_weight,
    v_scale,
    v_gain,
    spatial_weight,
    spatial_bias,
    out_weight,
    out_scale,
    gate_weight,
    gate_scale,
    up_weight,
    up_scale,
    down_weight,
    down_scale,
):
    local_rows = tokens.shape[0]
    out_columns, down_columns = turned_gather((out_scale, down_scale), "fs", (0, 0))
    u_whole, v_whole, out_whole = turned_gather(
        (
            u_weight.astype(jnp.bfloat16),
            v_weight.astype(jnp.bfloat16),
            out_weight.astype(jnp.bfloat16),
        ),
        "fs",
        (0, 0, 1),
    )
    normed = rms_rows(tokens, mix_gain)

    def project_mixer(segment, offset):
        u_pre = jnp.dot(segment, u_whole, preferred_element_type=jnp.float32) * u_scale
        v_pre = jnp.dot(segment, v_whole, preferred_element_type=jnp.float32) * v_scale
        return jnp.concatenate(
            [jax.nn.gelu(u_pre, approximate=True), jax.nn.gelu(v_pre, approximate=True)], axis=1
        ).astype(jnp.bfloat16)

    joined = collect_rows(normed, project_mixer)
    columns = u_whole.shape[1]
    u_values = joined[:, :columns]
    v_wide = joined[:, columns:].astype(jnp.float32)
    totals, squares = packed_total((jnp.sum(v_wide, axis=1), jnp.sum(v_wide * v_wide, axis=1)), TP)
    average = totals / A
    spread = squares / A - average * average
    v_normed = ((v_wide - average[:, None]) * lax.rsqrt(spread + 1e-05)[:, None] * v_gain).astype(
        jnp.bfloat16
    )
    group_dim = A // A_GROUPS
    groups = columns // group_dim
    first_group = lax.axis_index(TP) * groups
    weights = lax.dynamic_slice_in_dim(spatial_weight, first_group, groups, 0)
    offsets = lax.dynamic_slice_in_dim(spatial_bias, first_group, groups, 0)
    causal = jnp.tril(jnp.ones((BLK, BLK), dtype=bool))
    masked = jnp.where(causal[None], weights, jnp.zeros_like(weights))
    blocks = v_normed.reshape(-1, BLK, groups, group_dim)
    mixed_sum = jnp.einsum("gts,bsgd->btgd", masked, blocks, preferred_element_type=jnp.float32)
    mixed_sum = mixed_sum + offsets.T[None, :, :, None]
    gated_rows = (u_values.reshape(blocks.shape).astype(jnp.float32) * mixed_sum).astype(
        jnp.bfloat16
    )
    gated_rows = gated_rows.reshape(-1, columns)

    def mixer_term(offset, amount):
        return jnp.dot(gated_rows, out_whole, preferred_element_type=jnp.float32) * out_columns

    residual = (tokens.astype(jnp.float32) + reduce_rows(mixer_term, local_rows)).astype(
        jnp.bfloat16
    )
    gate_whole, up_whole, down_whole = turned_gather(
        (
            gate_weight.astype(jnp.bfloat16),
            up_weight.astype(jnp.bfloat16),
            down_weight.astype(jnp.bfloat16),
        ),
        "fs",
        (0, 0, 1),
    )
    normed_second = rms_rows(residual, ffn_gain)

    def project_ffn(segment, offset):
        gate_pre = jnp.dot(segment, gate_whole, preferred_element_type=jnp.float32) * gate_scale
        up_pre = jnp.dot(segment, up_whole, preferred_element_type=jnp.float32) * up_scale
        return (jax.nn.silu(gate_pre) * up_pre).astype(jnp.bfloat16)

    hidden = collect_rows(normed_second, project_ffn)

    def ffn_term(offset, amount):
        return jnp.dot(hidden, down_whole, preferred_element_type=jnp.float32) * down_columns

    return (residual.astype(jnp.float32) + reduce_rows(ffn_term, local_rows)).astype(jnp.bfloat16)


def solution(mesh):
    torus = Mesh(mesh.devices.reshape(mesh.shape["fs"], 4, 2), ("fs", "tp_0", "tp_1"))
    in_specs = (
        P(FS_TP, None),
        P(),
        P(),
        P("fs", TP),
        P(TP),
        P("fs", TP),
        P(TP),
        P(TP),
        P(),
        P(),
        P(TP, "fs"),
        P("fs"),
        P("fs", TP),
        P(TP),
        P("fs", TP),
        P(TP),
        P(TP, "fs"),
        P("fs"),
    )
    out_specs = P(FS_TP, None)
    return jax.shard_map(local, mesh=torus, in_specs=in_specs, out_specs=out_specs, check_vma=False)
```

profile of v0, /device:TPU:1, one launch (start us, length us, event | category | flops | bytes accessed | tf_op | source)
XLA Modules:
  0.0 238.5 jit_solution(4988067022852905276)
XLA Ops:
  11.5 1.2 copy.50
  15.0 1.6 broadcast_in_dim.13
  16.6 5.0 %all-to-all-start = ((bf16[4,128,2048]{2,1,0:T(8,128)(2,1)}), bf16[4,128,2048]{2,1,0:T(8,128)(2,1)S(1)}, u32[]{:S(2)}, u32[]{:S(2)}) async-start(bf16[4,128,2048]{2,1,0:T(8,128)(2,1)} %broadcast_in_dim.13), calls=%async_computation | async-start | bytes 4194304 | tf_op jit(solution)/shard_map/all_to_all | solution.py:16
  21.6 21.1 %all_gather.10 = f32[2048,2]{0,1:T(2,128)S(1)} all-gather(f32[128,2]{0,1:T(2,128)S(1)} %pad_maximum_fusion.3), channel_id=1, replica_groups=mesh['fs'=16,'tp_0'=4,'tp_1'=2] {'fs'}, dimensions={0}, use_global_device_ids=true | all-gather | bytes 17408 | tf_op jit(solution)/shard_map/all_gather | solution.py:56
  42.7 4.3 %all-to-all-done = bf16[4,128,2048]{2,1,0:T(8,128)(2,1)S(1)} async-done(((bf16[4,128,2048]{2,1,0:T(8,128)(2,1)}), bf16[4,128,2048]{2,1,0:T(8,128)(2,1)S(1)}, u32[]{:S(2)}, u32[]{:S(2)}) %all-to-all-start) | async-done | bytes 2097184 | tf_op jit(solution)/shard_map/all_to_all | solution.py:16
  47.6 8.5 %all_to_all.46 = bf16[2,4,128,2048]{3,2,1,0:T(8,128)(2,1)S(1)} all-to-all(bf16[2,4,128,2048]{3,2,1,0:T(8,128)(2,1)S(1)} %broadcast_in_dim.14), channel_id=1, replica_groups=mesh['fs'=16,'tp_0'=4,'tp_1'=2] {'tp_1'}, dimensions={0} | all-to-all | bytes 8388608 | tf_op jit(solution)/shard_map/all_to_all | solution.py:16
  56.1 2.4 copy.43
  58.5 5.7 %all-gather.3.cloned.1.call-done = bf16[2048,768]{0,1:T(8,128)(2,1)} async-done(((bf16[128,768]{0,1:T(8,128)(2,1)}), bf16[2048,768]{0,1:T(8,128)(2,1)}) %all-gather.3.cloned.1.call-update) | async-done | bytes 3145744 | tf_op jit(solution)/shard_map/all_gather | solution.py:56
  64.2 4.1 %convert_reduce_fusion.2 = (f32[1024]{0:T(1024)S(1)}, f32[1024]{0:T(1024)S(1)}, bf16[1024,256]{1,0:T(8,128)(2,1)S(1)}) fusion(f32[256]{0:T(256)S(1)} %copy-done.10, bf16[1024,2048]{1,0:T(8,128)(2,1)} %bitcast.56, bf16[2048,768]{0,1:T(8,128)(2,1)} %all-gather.3.cloned.1.call-done), kind=kOutput, calls=%fused_computation.17 | convolution fusion | flops 1077409792 | bytes 5776384 | tf_op jit(solution)/shard_map/dot_general | solution.py:130
  69.1 6.3 %all-to-all-start.2 = ((f32[8,1,2048]{2,1,0:T(1,128)}), f32[8,1,2048]{2,1,0:T(1,128)S(1)}, u32[]{:S(2)}, u32[]{:S(2)}) async-start(f32[8,1,2048]{2,1,0:T(1,128)} %broadcast_in_dim.15), calls=%async_computation.2 | async-start | bytes 131072 | tf_op jit(solution)/shard_map/all_to_all | solution.py:16
  75.4 4.4 %fusion.24 = bf16[1024,256]{1,0:T(8,128)(2,1)S(1)} fusion(bf16[1024,2048]{1,0:T(8,128)(2,1)} %bitcast.57, bf16[2048,768]{0,1:T(8,128)(2,1)} %all-gather.3.cloned.1.call-done, f32[256]{0:T(256)S(1)} %copy-done.11), kind=kOutput, calls=%fused_computation.41 | convolution fusion | flops 1076363264 | bytes 5768192 | tf_op jit(solution)/shard_map/dot_general | solution.py:129
  81.7 2.5 %multiply_convert_fusion.1 = bf16[1024,2048]{1,0:T(8,128)(2,1)S(1)} fusion(bf16[1024,256]{1,0:T(8,128)(2,1)S(1)} %bitcast.64, f32[2048]{0:T(1024)S(1)} %bitcast.66, bf16[2048,768]{0,1:T(8,128)(2,1)} %all-gather.3.cloned.1.call-done), kind=kOutput, calls=%fused_computation.1 | convolution fusion | flops 1077936128 | bytes 5775360 | tf_op jit(solution)/shard_map/dot_general | solution.py:161
  84.8 8.5 %all_to_all.47 = bf16[2,4,128,2048]{3,2,1,0:T(8,128)(2,1)} all-to-all(bf16[2,4,128,2048]{3,2,1,0:T(8,128)(2,1)S(1)} %bitcast.54), channel_id=1, replica_groups=mesh['fs'=16,'tp_0'=4,'tp_1'=2] {'tp_1'}, dimensions={0} | all-to-all | bytes 8388608 | tf_op jit(solution)/shard_map/all_to_all | solution.py:41
  93.3 3.5 %reduce_sum.91 = bf16[4,128,2048]{2,1,0:T(8,128)(2,1)S(1)} reduce(bf16[2,4,128,2048]{3,2,1,0:T(8,128)(2,1)} %all_to_all.47, bf16[]{:T(256)} %constant.43.clone.1), dimensions={0}, to_apply=%region_4.5 | reduce | flops 1048576 | bytes 6291458 | tf_op jit(solution)/shard_map/reduce_sum | solution.py:42
  96.9 28.6 %all_to_all.48 = bf16[4,128,2048]{2,1,0:T(8,128)(2,1)S(1)} all-to-all(bf16[4,128,2048]{2,1,0:T(8,128)(2,1)S(1)} %reduce_sum.91), channel_id=1, replica_groups=mesh['fs'=16,'tp_0'=4,'tp_1'=2] {'tp_0'}, dimensions={0} | all-to-all | bytes 4194304 | tf_op jit(solution)/shard_map/all_to_all | solution.py:49
  126.6 27.1 %all_to_all.49 = bf16[4,128,2048]{2,1,0:T(8,128)(2,1)S(1)} all-to-all(bf16[4,128,2048]{2,1,0:T(8,128)(2,1)S(1)} %broadcast_in_dim.17), channel_id=1, replica_groups=mesh['fs'=16,'tp_0'=4,'tp_1'=2] {'tp_0'}, dimensions={0} | all-to-all | bytes 4194304 | tf_op jit(solution)/shard_map/all_to_all | solution.py:16
  154.2 9.4 %all_to_all.50 = bf16[2,4,128,2048]{3,2,1,0:T(8,128)(2,1)S(1)} all-to-all(bf16[2,4,128,2048]{3,2,1,0:T(8,128)(2,1)S(1)} %broadcast_in_dim.18), channel_id=1, replica_groups=mesh['fs'=16,'tp_0'=4,'tp_1'=2] {'tp_1'}, dimensions={0} | all-to-all | bytes 8388608 | tf_op jit(solution)/shard_map/all_to_all | solution.py:16
  163.7 2.4 copy.48
  166.1 8.2 %fusion.1 = f32[1024,768]{1,0:T(8,128)} fusion(bf16[1024,2048]{1,0:T(8,128)(2,1)} %bitcast.58, bf16[2048,2304]{0,1:T(8,128)(2,1)} %all-gather.5.cloned.1.call-done), kind=kOutput, calls=%fused_computation.7 | convolution fusion | flops 3221225472 | bytes 10485760 | tf_op jit(solution)/shard_map/dot_general | solution.py:179
  174.3 13.4 %multiply_convert_fusion = bf16[1024,2048]{1,0:T(8,128)(2,1)} fusion(f32[2048]{0:T(1024)S(1)} %bitcast.65, bf16[2048,2304]{0,1:T(8,128)(2,1)} %all-gather.5.cloned.1.call-done, f32[1024,768]{1,0:T(8,128)} %fusion.1, bf16[1024,2048]{1,0:T(8,128)(2,1)} %bitcast.59, f32[768]{0:T(1024)S(1)} %copy-done.8, f32[768]{0:T(1024)S(1)} %copy-done.9), kind=kOutput, calls=%fused_computation | convolution fusion | flops 6452936704 | bytes 17840128 | tf_op jit(solution)/shard_map/dot_general | solution.py:185
  187.7 2.5 %copy.57 = bf16[4,2,128,2048]{3,2,0,1:T(8,128)(2,1)S(1)} copy(bf16[4,2,128,2048]{3,2,1,0:T(8,128)(2,1)} %bitcast.60) | data formatting | bytes 8388608 | tf_op jit(solution)/shard_map/reshape;reshape | solution.py:35
  190.2 8.1 %all_to_all.51 = bf16[2,4,128,2048]{3,2,1,0:T(8,128)(2,1)} all-to-all(bf16[2,4,128,2048]{3,2,1,0:T(8,128)(2,1)S(1)} %bitcast.55), channel_id=1, replica_groups=mesh['fs'=16,'tp_0'=4,'tp_1'=2] {'tp_1'}, dimensions={0} | all-to-all | bytes 8388608 | tf_op jit(solution)/shard_map/all_to_all | solution.py:41
  198.3 3.5 %reduce_sum.94 = bf16[4,128,2048]{2,1,0:T(8,128)(2,1)S(1)} reduce(bf16[2,4,128,2048]{3,2,1,0:T(8,128)(2,1)} %all_to_all.51, bf16[]{:T(256)} %constant.43.clone.1), dimensions={0}, to_apply=%region_7.8 | reduce | flops 1048576 | bytes 6291458 | tf_op jit(solution)/shard_map/reduce_sum | solution.py:42
  201.9 28.5 %all_to_all.52 = bf16[4,128,2048]{2,1,0:T(8,128)(2,1)S(1)} all-to-all(bf16[4,128,2048]{2,1,0:T(8,128)(2,1)S(1)} %reduce_sum.94), channel_id=1, replica_groups=mesh['fs'=16,'tp_0'=4,'tp_1'=2] {'tp_0'}, dimensions={0} | all-to-all | bytes 4194304 | tf_op jit(solution)/shard_map/all_to_all | solution.py:49
  (59 shorter events, 13.9 us)
Async XLA Ops:
  6.5 36.1 %copy-start = (f32[8,128]{1,0:T(8,128)S(1)}, f32[8,128]{1,0:T(8,128)}, u32[]{:S(2)}) copy-start(f32[8,128]{1,0:T(8,128)} %param.27) | copy-start | bytes 12292
  6.5 8.0 %copy-start.2 = (bf16[128,2048]{1,0:T(8,128)(2,1)S(1)}, bf16[128,2048]{1,0:T(8,128)(2,1)}, u32[]{:S(2)}) copy-start(bf16[128,2048]{1,0:T(8,128)(2,1)} %param.18) | copy-start | bytes 1572868
  6.5 8.2 %copy-start.3 = (f32[2048]{0:T(1024)S(1)}, f32[2048]{0:T(1024)}, u32[]{:S(2)}) copy-start(f32[2048]{0:T(1024)} %param.19) | copy-start | bytes 24580
  6.5 57.7 %all-gather.3.cloned.1.call-start = ((), (), s32[]{:S(2)}) async-start(), calls=%async_computation.9 | async-start | bytes 3342336 | tf_op jit(solution)/shard_map/all_gather | solution.py:56
  10.3 155.8 %all-gather.5.cloned.1.call-start = ((), (), s32[]{:S(2)}) async-start(), calls=%async_computation.10 | async-start | bytes 10027008 | tf_op jit(solution)/shard_map/all_gather | solution.py:56
  15.0 6.6 %copy-start.6 = (f32[128]{0:T(128)S(1)}, f32[128]{0:T(128)}, u32[]{:S(2)}) copy-start(f32[128]{0:T(128)} %param.35) | copy-start | bytes 1540
  15.0 6.6 %copy-start.7 = (f32[128]{0:T(128)S(1)}, f32[128]{0:T(128)}, u32[]{:S(2)}) copy-start(f32[128]{0:T(128)} %param.29) | copy-start | bytes 1540
  16.6 30.5 %all-to-all-start = ((bf16[4,128,2048]{2,1,0:T(8,128)(2,1)}), bf16[4,128,2048]{2,1,0:T(8,128)(2,1)S(1)}, u32[]{:S(2)}, u32[]{:S(2)}) async-start(bf16[4,128,2048]{2,1,0:T(8,128)(2,1)} %broadcast_in_dim.13), calls=%async_computation | async-start | bytes 4194304 | tf_op jit(solution)/shard_map/all_to_all | solution.py:16
  56.1 8.1 %copy-start.10 = (f32[256]{0:T(256)S(1)}, f32[256]{0:T(256)}, u32[]{:S(2)}) copy-start(f32[256]{0:T(256)} %param.24) | copy-start | bytes 3076
  64.2 11.2 %copy-start.11 = (f32[256]{0:T(256)S(1)}, f32[256]{0:T(256)}, u32[]{:S(2)}) copy-start(f32[256]{0:T(256)} %param.22) | copy-start | bytes 3076
  69.1 11.2 %all-to-all-start.2 = ((f32[8,1,2048]{2,1,0:T(1,128)}), f32[8,1,2048]{2,1,0:T(1,128)S(1)}, u32[]{:S(2)}, u32[]{:S(2)}) async-start(f32[8,1,2048]{2,1,0:T(1,128)} %broadcast_in_dim.15), calls=%async_computation.2 | async-start | bytes 131072 | tf_op jit(solution)/shard_map/all_to_all | solution.py:16
  75.4 4.9 %copy-start.5 = (f32[256]{0:T(256)S(1)}, f32[256]{0:T(256)}, u32[]{:S(2)}) copy-start(f32[256]{0:T(256)} %param.25) | copy-start | bytes 3076
  125.5 0.7 copy-start.4
  166.1 8.2 %copy-start.8 = (f32[768]{0:T(1024)S(1)}, f32[768]{0:T(1024)}, u32[]{:S(2)}) copy-start(f32[768]{0:T(1024)} %param.33) | copy-start | bytes 9220
  166.1 8.2 %copy-start.9 = (f32[768]{0:T(1024)S(1)}, f32[768]{0:T(1024)}, u32[]{:S(2)}) copy-start(f32[768]{0:T(1024)} %param.31) | copy-start | bytes 9220
  201.8 29.9 %copy-start.1 = (f32[8,128]{1,0:T(8,128)S(1)}, f32[8,128]{1,0:T(8,128)}, u32[]{:S(2)}) copy-start(f32[8,128]{1,0:T(8,128)} %param.27) | copy-start | bytes 12292
Sparse Core Ops, SparseCore 0:
  10.4 53.7 all-gather.2
  66.3 81.8 all-gather.4
where the time goes:
time: 240 us; the launch traced here: 239 us
  blocking collectives  140 us (58%)
  matrix products  33.7 us (14%)
  local copies, waits for them, and re-layouts  15.9 us (7%)
  between operations  13.6 us (6%)
  other arithmetic  13.5 us (6%)
  starting transfers between devices  11.4 us (5%)
  waiting for transfers between devices  10.6 us (4%)
    all_to_all x2, blocking collectives, sum_in_two_steps(): lax.all_to_all(own.astype(jnp.bfloat16), far, 0, 0, tiled=True)  57.1 us
    all_to_all x3, blocking collectives, copy_for_each(): lax.all_to_all(jnp.broadcast_to(value[None], (peers, *value.shape)), axis...  45.1 us
    all_gather x1, blocking collectives, turned_gather(): out, at, finished = (lax.all_gather(both, axis, axis=0, tiled=True), 0, [])  21.1 us
    all_to_all x2, blocking collectives, sent_and_summed(): lax.all_to_all(tiles, axis, split_axis=0, concat_axis=0, tiled=True)  16.7 us
    dot_general x1, matrix products, ffn_term(): jnp.dot(hidden, down_whole, preferred_element_type=jnp.float32)  13.4 us
    all_to_all x2, starting transfers between devices, copy_for_each(): lax.all_to_all(jnp.broadcast_to(value[None], (peers, *value.shape)), axis...  11.3 us
    dot_general x1, matrix products, project_ffn(): jnp.dot(segment, up_whole, preferred_element_type=jnp.float32) * up_scale  8.24 us
    reduce_sum x2, other arithmetic, sent_and_summed(): return arrived.astype(jnp.float32).sum(axis=0)  7.1 us
  transfers between devices with their start and end apart: 4, of which 3 were waited for; matrix products, arithmetic and copies ran while one was open for 13% of the time, Pallas kernels for 0%

commit v1 on v0

--- a/solution.py
+++ b/solution.py
@@ -53,7 +53,20 @@
 def turned_gather(arrays, axis, dims):
     turned = [jnp.moveaxis(a, dim, 0) for a, dim in zip(arrays, dims)]
     both = jnp.concatenate([t.reshape(len(t), -1) for t in turned], axis=1)
-    out, at, finished = (lax.all_gather(both, axis, axis=0, tiled=True), 0, [])
+
+    def obtain_map_by_axis(my_tile):
+        current_arr = jnp.concatenate(
+            jax.lax.all_to_all(
+                jnp.stack(jax.lax.axis_size(axis) * [my_tile], axis=0),
+                axis_name=axis,
+                split_axis=0,
+                concat_axis=0,
+            ),
+            0,
+        )
+        return current_arr
+
+    out, at, finished = (obtain_map_by_axis(both), 0, [])
     for t, dim in zip(turned, dims):
         piece = out[:, at : at + t[0].size].reshape(-1, *t.shape[1:])
         finished.append(jnp.moveaxis(piece, 0, dim))

time: 240 us -> 432 us (1.80)
  waiting for transfers between devices: 10.6 us -> 228 us
  blocking collectives: 140 us -> 96.3 us
  starting transfers between devices: 11.4 us -> 29.4 us
  between operations: 13.6 us -> 0.32 us
  local copies, waits for them, and re-layouts: 15.9 us -> 27.8 us
    all_to_all x0 -> x3, waiting for transfers between devices: none -> 184 us  [obtain_map_by_axis(): jax.lax.all_to_all(jnp.stack(jax.lax.axis_size(axis) * [my_tile], axis=0)...]
    all_to_all x2 -> x3, waiting for transfers between devices: 4.82 us -> 44.1 us  [copy_for_each(): lax.all_to_all(jnp.broadcast_to(value[None], (peers, *value.shape)), axis...]
    all_to_all x3 -> x2, blocking collectives: 45.1 us -> 21.5 us  [copy_for_each(): lax.all_to_all(jnp.broadcast_to(value[None], (peers, *value.shape)), axis...]
    all_gather x1 -> x0, blocking collectives: 21.1 us -> none  [turned_gather(): out, at, finished = (lax.all_gather(both, axis, axis=0, tiled=True), 0, [])]
    all_to_all x0 -> x3, starting transfers between devices: none -> 17.1 us  [obtain_map_by_axis(): jax.lax.all_to_all(jnp.stack(jax.lax.axis_size(axis) * [my_tile], axis=0)...]
    another operation x0 -> x3, local copies, waits for them, and re-layouts: none -> 7.22 us  [obtain_map_by_axis(): jnp.stack(jax.lax.axis_size(axis) * [my_tile], axis=0)]
    all_gather x2 -> x0, waiting for transfers between devices: 5.74 us -> none  [turned_gather(): out, at, finished = (lax.all_gather(both, axis, axis=0, tiled=True), 0, [])]
    all_to_all x2, local copies, waits for them, and re-layouts: 4.76 us -> 9.5 us  [copy_for_each(): lax.all_to_all(jnp.broadcast_to(value[None], (peers, *value.shape)), axis...]
  transfers between devices with their start and end apart: 4 -> 6, of which waited for: 3 -> 6; matrix products, arithmetic and copies ran while one was open for 13% -> 5% of each run, Pallas kernels for 0% -> 0%
where the time goes in v1:
time: 432 us; the launch traced here: 431 us
  waiting for transfers between devices  228 us (53%)
  blocking collectives  96.3 us (22%)
  matrix products  33.1 us (8%)
  starting transfers between devices  29.4 us (7%)
  local copies, waits for them, and re-layouts  27.8 us (6%)
  other arithmetic  15.7 us (4%)
    all_to_all x3, waiting for transfers between devices, obtain_map_by_axis(): jax.lax.all_to_all(jnp.stack(jax.lax.axis_size(axis) * [my_tile], axis=0)...  184 us
    all_to_all x2, blocking collectives, sum_in_two_steps(): lax.all_to_all(own.astype(jnp.bfloat16), far, 0, 0, tiled=True)  57.3 us
    all_to_all x3, waiting for transfers between devices, copy_for_each(): lax.all_to_all(jnp.broadcast_to(value[None], (peers, *value.shape)), axis...  44.1 us
    all_to_all x2, blocking collectives, copy_for_each(): lax.all_to_all(jnp.broadcast_to(value[None], (peers, *value.shape)), axis...  21.5 us
    all_to_all x2, blocking collectives, sent_and_summed(): lax.all_to_all(tiles, axis, split_axis=0, concat_axis=0, tiled=True)  17.6 us
    all_to_all x3, starting transfers between devices, obtain_map_by_axis(): jax.lax.all_to_all(jnp.stack(jax.lax.axis_size(axis) * [my_tile], axis=0)...  17.1 us
    dot_general x1, matrix products, ffn_term(): jnp.dot(hidden, down_whole, preferred_element_type=jnp.float32)  13.3 us
    all_to_all x3, starting transfers between devices, copy_for_each(): lax.all_to_all(jnp.broadcast_to(value[None], (peers, *value.shape)), axis...  12.3 us
  transfers between devices with their start and end apart: 6, of which 6 were waited for; matrix products, arithmetic and copies ran while one was open for 5% of the time, Pallas kernels for 0%

profile of v1, /device:TPU:1, one launch (start us, length us, event | category | flops | bytes accessed | tf_op | source)
XLA Modules:
  0.0 430.6 jit_solution(3424249766580630812)
XLA Ops:
  1.3 8.4 %all-to-all-start.4 = ((f32[16,128,2]{1,2,0:T(2,128)}), f32[16,128,2]{1,2,0:T(2,128)S(1)}, u32[]{:S(2)}, u32[]{:S(2)}) async-start(f32[16,128,2]{1,2,0:T(2,128)} %stack.7), calls=%async_computation.4 | async-start | bytes 32768 | tf_op jit(solution)/shard_map/all_to_all | solution.py:59
  12.2 3.9 all-to-all-done.4
  17.8 4.2 all-to-all-start
  22.4 23.6 %all-to-all-done = bf16[4,128,2048]{2,1,0:T(8,128)(2,1)S(1)} async-done(((bf16[4,128,2048]{2,1,0:T(8,128)(2,1)}), bf16[4,128,2048]{2,1,0:T(8,128)(2,1)S(1)}, u32[]{:S(2)}, u32[]{:S(2)}) %all-to-all-start) | async-done | bytes 2097184 | tf_op jit(solution)/shard_map/all_to_all | solution.py:16
  46.5 11.0 %all_to_all.61 = bf16[2,4,128,2048]{3,2,1,0:T(8,128)(2,1)} all-to-all(bf16[2,4,128,2048]{3,2,1,0:T(8,128)(2,1)S(1)} %broadcast_in_dim.14), channel_id=1, replica_groups=mesh['fs'=16,'tp_0'=4,'tp_1'=2] {'tp_1'}, dimensions={0} | all-to-all | bytes 8388608 | tf_op jit(solution)/shard_map/all_to_all | solution.py:16
  59.6 3.7 all-to-all-start.2
  63.4 4.7 %copy.52 = bf16[2,4,128,2048]{3,2,0,1:T(8,128)(2,1)} copy(bf16[2,4,128,2048]{3,2,1,0:T(8,128)(2,1)} %all_to_all.61) | data formatting | bytes 8388608 | tf_op jit(solution)/shard_map/all_to_all | solution.py:16
  68.1 43.3 %all-to-all-done.2 = bf16[16,128,768]{2,1,0:T(8,128)(2,1)S(1)} async-done(((bf16[16,128,768]{2,1,0:T(8,128)(2,1)}), bf16[16,128,768]{2,1,0:T(8,128)(2,1)S(1)}, u32[]{:S(2)}, u32[]{:S(2)}) %all-to-all-start.2) | async-done | bytes 3145760 | tf_op jit(solution)/shard_map/all_to_all | solution.py:59
  111.5 4.5 %convert_reduce_fusion.2 = (f32[1024]{0:T(1024)S(1)}, f32[1024]{0:T(1024)S(1)}, bf16[1024,256]{1,0:T(8,128)(2,1)}) fusion(f32[256]{0:T(256)S(1)} %copy-done.11, bf16[1024,2048]{1,0:T(8,128)(2,1)} %bitcast.59, bf16[2048,768]{1,0:T(8,128)(2,1)S(1)} %bitcast.65), kind=kOutput, calls=%fused_computation.17 | convolution fusion | flops 1077409792 | bytes 5776384 | tf_op jit(solution)/shard_map/dot_general | solution.py:143
  116.6 4.5 %all-to-all-start.3 = ((f32[8,1,2048]{2,1,0:T(1,128)}), f32[8,1,2048]{2,1,0:T(1,128)S(1)}, u32[]{:S(2)}, u32[]{:S(2)}) async-start(f32[8,1,2048]{2,1,0:T(1,128)} %broadcast_in_dim.15), calls=%async_computation.3 | async-start | bytes 131072 | tf_op jit(solution)/shard_map/all_to_all | solution.py:16
  121.1 4.4 %fusion.24 = bf16[1024,256]{1,0:T(8,128)(2,1)} fusion(bf16[1024,2048]{1,0:T(8,128)(2,1)} %bitcast.60, bf16[2048,768]{1,0:T(8,128)(2,1)S(1)} %bitcast.66, f32[256]{0:T(256)S(1)} %copy-done.12), kind=kOutput, calls=%fused_computation.41 | convolution fusion | flops 1076363264 | bytes 5768192 | tf_op jit(solution)/shard_map/dot_general | solution.py:142
  130.7 8.6 %all_to_all.62 = bf16[2,4,128,2048]{3,2,1,0:T(8,128)(2,1)} all-to-all(bf16[2,4,128,2048]{3,2,1,0:T(8,128)(2,1)S(1)} %bitcast.57), channel_id=1, replica_groups=mesh['fs'=16,'tp_0'=4,'tp_1'=2] {'tp_1'}, dimensions={0} | all-to-all | bytes 8388608 | tf_op jit(solution)/shard_map/all_to_all | solution.py:41
  142.8 28.7 %all_to_all.63 = bf16[4,128,2048]{2,1,0:T(8,128)(2,1)S(1)} all-to-all(bf16[4,128,2048]{2,1,0:T(8,128)(2,1)S(1)} %reduce_sum.91), channel_id=1, replica_groups=mesh['fs'=16,'tp_0'=4,'tp_1'=2] {'tp_0'}, dimensions={0} | all-to-all | bytes 4194304 | tf_op jit(solution)/shard_map/all_to_all | solution.py:49
  174.1 3.6 all-to-all-start.7
  182.2 20.1 %all-to-all-done.7 = bf16[4,128,2048]{2,1,0:T(8,128)(2,1)S(1)} async-done(((bf16[4,128,2048]{2,1,0:T(8,128)(2,1)}), bf16[4,128,2048]{2,1,0:T(8,128)(2,1)S(1)}, u32[]{:S(2)}, u32[]{:S(2)}) %all-to-all-start.7) | async-done | bytes 2097184 | tf_op jit(solution)/shard_map/all_to_all | solution.py:16
  202.8 10.5 %all_to_all.64 = bf16[2,4,128,2048]{3,2,1,0:T(8,128)(2,1)} all-to-all(bf16[2,4,128,2048]{3,2,1,0:T(8,128)(2,1)S(1)} %broadcast_in_dim.18), channel_id=1, replica_groups=mesh['fs'=16,'tp_0'=4,'tp_1'=2] {'tp_1'}, dimensions={0} | all-to-all | bytes 8388608 | tf_op jit(solution)/shard_map/all_to_all | solution.py:16
  213.3 4.6 %stack.8 = bf16[16,128,2304]{2,1,0:T(8,128)(2,1)} broadcast(bf16[128,2304]{1,0:T(8,128)(2,1)S(1)} %copy.61), dimensions={1,2} | broadcast | bytes 10027008 | tf_op jit(solution)/shard_map/stack | solution.py:60
  217.8 5.0 %all-to-all-start.9 = ((bf16[16,128,2304]{2,1,0:T(8,128)(2,1)}), bf16[16,128,2304]{2,1,0:T(8,128)(2,1)}, u32[]{:S(2)}, u32[]{:S(2)}) async-start(bf16[16,128,2304]{2,1,0:T(8,128)(2,1)} %stack.8), calls=%async_computation.9 | async-start | bytes 18874368 | tf_op jit(solution)/shard_map/all_to_all | solution.py:59
  222.8 4.8 %copy.58 = bf16[2,4,128,2048]{3,2,0,1:T(8,128)(2,1)} copy(bf16[2,4,128,2048]{3,2,1,0:T(8,128)(2,1)} %all_to_all.64) | data formatting | bytes 8388608 | tf_op jit(solution)/shard_map/all_to_all | solution.py:16
  227.6 136.6 %all-to-all-done.9 = bf16[16,128,2304]{2,1,0:T(8,128)(2,1)} async-done(((bf16[16,128,2304]{2,1,0:T(8,128)(2,1)}), bf16[16,128,2304]{2,1,0:T(8,128)(2,1)}, u32[]{:S(2)}, u32[]{:S(2)}) %all-to-all-start.9) | async-done | bytes 9437216 | tf_op jit(solution)/shard_map/all_to_all | solution.py:59
  364.1 8.2 %fusion.1 = f32[1024,768]{1,0:T(8,128)} fusion(bf16[1024,2048]{1,0:T(8,128)(2,1)} %bitcast.61, bf16[2048,2304]{1,0:T(8,128)(2,1)} %bitcast.22), kind=kOutput, calls=%fused_computation.7 | convolution fusion | flops 3221225472 | bytes 10485760 | tf_op jit(solution)/shard_map/dot_general | solution.py:192
  372.4 13.3 %multiply_convert_fusion = bf16[1024,2048]{1,0:T(8,128)(2,1)} fusion(f32[2048]{0:T(1024)S(1)} %bitcast.72, bf16[2048,2304]{1,0:T(8,128)(2,1)} %bitcast.22, f32[1024,768]{1,0:T(8,128)} %fusion.1, bf16[1024,2048]{1,0:T(8,128)(2,1)} %bitcast.62, f32[768]{0:T(1024)S(1)} %copy-done.9, f32[768]{0:T(1024)S(1)} %copy-done.10), kind=kOutput, calls=%fused_computation | convolution fusion | flops 6452936704 | bytes 17840128 | tf_op jit(solution)/shard_map/dot_general | solution.py:198
  388.2 9.0 %all_to_all.65 = bf16[2,4,128,2048]{3,2,1,0:T(8,128)(2,1)} all-to-all(bf16[2,4,128,2048]{3,2,1,0:T(8,128)(2,1)S(1)} %bitcast.58), channel_id=1, replica_groups=mesh['fs'=16,'tp_0'=4,'tp_1'=2] {'tp_1'}, dimensions={0} | all-to-all | bytes 8388608 | tf_op jit(solution)/shard_map/all_to_all | solution.py:41
  400.8 28.5 %all_to_all.66 = bf16[4,128,2048]{2,1,0:T(8,128)(2,1)S(1)} all-to-all(bf16[4,128,2048]{2,1,0:T(8,128)(2,1)S(1)} %reduce_sum.94), channel_id=1, replica_groups=mesh['fs'=16,'tp_0'=4,'tp_1'=2] {'tp_0'}, dimensions={0} | all-to-all | bytes 4194304 | tf_op jit(solution)/shard_map/all_to_all | solution.py:49
  (66 shorter events, 32.6 us)
Async XLA Ops:
  0.0 63.4 %copy-start = (f32[8,128]{1,0:T(8,128)S(1)}, f32[8,128]{1,0:T(8,128)}, u32[]{:S(2)}) copy-start(f32[8,128]{1,0:T(8,128)} %param.27) | copy-start | bytes 12292
  1.3 14.9 %all-to-all-start.4 = ((f32[16,128,2]{1,2,0:T(2,128)}), f32[16,128,2]{1,2,0:T(2,128)S(1)}, u32[]{:S(2)}, u32[]{:S(2)}) async-start(f32[16,128,2]{1,2,0:T(2,128)} %stack.7), calls=%async_computation.4 | async-start | bytes 32768 | tf_op jit(solution)/shard_map/all_to_all | solution.py:59
  12.2 9.8 %copy-start.4 = (f32[128,256]{1,0:T(8,128)S(1)}, f32[128,256]{1,0:T(8,128)}, u32[]{:S(2)}) copy-start(f32[128,256]{1,0:T(8,128)} %param.23) | copy-start | bytes 393220
  12.2 9.9 %copy-start.5 = (f32[128,256]{1,0:T(8,128)S(1)}, f32[128,256]{1,0:T(8,128)}, u32[]{:S(2)}) copy-start(f32[128,256]{1,0:T(8,128)} %param.21) | copy-start | bytes 393220
  12.2 10.0 %copy-start.6 = (f32[256,128]{1,0:T(8,128)S(1)}, f32[256,128]{1,0:T(8,128)}, u32[]{:S(2)}) copy-start(f32[256,128]{1,0:T(8,128)} %param.28) | copy-start | bytes 393220
  17.8 28.2 %all-to-all-start = ((bf16[4,128,2048]{2,1,0:T(8,128)(2,1)}), bf16[4,128,2048]{2,1,0:T(8,128)(2,1)S(1)}, u32[]{:S(2)}, u32[]{:S(2)}) async-start(bf16[4,128,2048]{2,1,0:T(8,128)(2,1)} %broadcast_in_dim.13), calls=%async_computation | async-start | bytes 4194304 | tf_op jit(solution)/shard_map/all_to_all | solution.py:16
  59.6 51.9 %all-to-all-start.2 = ((bf16[16,128,768]{2,1,0:T(8,128)(2,1)}), bf16[16,128,768]{2,1,0:T(8,128)(2,1)S(1)}, u32[]{:S(2)}, u32[]{:S(2)}) async-start(bf16[16,128,768]{2,1,0:T(8,128)(2,1)} %stack.6), calls=%async_computation.2 | async-start | bytes 6291456 | tf_op jit(solution)/shard_map/all_to_all | solution.py:59
  63.4 48.1 %copy-start.11 = (f32[256]{0:T(256)S(1)}, f32[256]{0:T(256)}, u32[]{:S(2)}) copy-start(f32[256]{0:T(256)} %param.24) | copy-start | bytes 3076
  111.5 9.6 %copy-start.12 = (f32[256]{0:T(256)S(1)}, f32[256]{0:T(256)}, u32[]{:S(2)}) copy-start(f32[256]{0:T(256)} %param.22) | copy-start | bytes 3076
  116.6 9.4 %all-to-all-start.3 = ((f32[8,1,2048]{2,1,0:T(1,128)}), f32[8,1,2048]{2,1,0:T(1,128)S(1)}, u32[]{:S(2)}, u32[]{:S(2)}) async-start(f32[8,1,2048]{2,1,0:T(1,128)} %broadcast_in_dim.15), calls=%async_computation.3 | async-start | bytes 131072 | tf_op jit(solution)/shard_map/all_to_all | solution.py:16
  121.1 4.9 %copy-start.8 = (f32[256]{0:T(256)S(1)}, f32[256]{0:T(256)}, u32[]{:S(2)}) copy-start(f32[256]{0:T(256)} %param.25) | copy-start | bytes 3076
  142.8 29.1 %copy-start.2 = (bf16[128,2048]{1,0:T(8,128)(2,1)S(1)}, bf16[128,2048]{1,0:T(8,128)(2,1)}, u32[]{:S(2)}) copy-start(bf16[128,2048]{1,0:T(8,128)(2,1)} %param.18) | copy-start | bytes 1572868
  171.6 0.7 copy-start.7
  172.5 5.2 %copy-start.3 = (f32[128,768]{1,0:T(8,128)S(1)}, f32[128,768]{1,0:T(8,128)}, u32[]{:S(2)}) copy-start(f32[128,768]{1,0:T(8,128)} %param.32) | copy-start | bytes 1179652
  174.1 28.2 %all-to-all-start.7 = ((bf16[4,128,2048]{2,1,0:T(8,128)(2,1)}), bf16[4,128,2048]{2,1,0:T(8,128)(2,1)S(1)}, u32[]{:S(2)}, u32[]{:S(2)}) async-start(bf16[4,128,2048]{2,1,0:T(8,128)(2,1)} %broadcast_in_dim.17), calls=%async_computation.7 | async-start | bytes 4194304 | tf_op jit(solution)/shard_map/all_to_all | solution.py:16
  217.8 146.3 %all-to-all-start.9 = ((bf16[16,128,2304]{2,1,0:T(8,128)(2,1)}), bf16[16,128,2304]{2,1,0:T(8,128)(2,1)}, u32[]{:S(2)}, u32[]{:S(2)}) async-start(bf16[16,128,2304]{2,1,0:T(8,128)(2,1)} %stack.8), calls=%async_computation.9 | async-start | bytes 18874368 | tf_op jit(solution)/shard_map/all_to_all | solution.py:59
  364.1 8.2 %copy-start.9 = (f32[768]{0:T(1024)S(1)}, f32[768]{0:T(1024)}, u32[]{:S(2)}) copy-start(f32[768]{0:T(1024)} %param.33) | copy-start | bytes 9220
  364.1 8.2 %copy-start.10 = (f32[768]{0:T(1024)S(1)}, f32[768]{0:T(1024)}, u32[]{:S(2)}) copy-start(f32[768]{0:T(1024)} %param.31) | copy-start | bytes 9220
  400.8 29.9 %copy-start.1 = (f32[8,128]{1,0:T(8,128)S(1)}, f32[8,128]{1,0:T(8,128)}, u32[]{:S(2)}) copy-start(f32[8,128]{1,0:T(8,128)} %param.27) | copy-start | bytes 12292
